TPU v7x, 256 devices: a whole 4x4x8 slice. The times are simulated.
256 devices in a mesh: sp: 64 (over z, y, core), tp: 4 (over x).
Axes of the slice: x: 4, y: 4, z: 8, core: 2. Of those that a mesh axis runs over, the one named last changes fastest.
Arguments:
- tokens: bfloat16 [24576, 2048], P('sp', 'tp'), may hold values from -6 to 6
- norm_gain: float32 [3, 2048], replicated, may hold values from 0.1 to 1.9
- w_value: bfloat16 [3, 2048, 1024], P(None, 'sp', 'tp'), may hold values from -0.125 to 0.125
- w_gate: bfloat16 [3, 2048, 1024], P(None, 'sp', 'tp'), may hold values from -0.125 to 0.125
- conv_taps: float32 [3, 31, 1024], P(None, None, 'tp'), may hold values from -2.4 to 2.4
- conv_bias: float32 [3, 1024], P(None, 'tp'), may hold values from -3 to 3
- ln_gain: float32 [3, 1024], P(None, 'tp'), may hold values from 0.1 to 1.9
- ln_shift: float32 [3, 1024], P(None, 'tp'), may hold values from -3 to 3
- w_out: bfloat16 [3, 1024, 2048], P(None, 'tp', 'sp'), may hold values from -0.1875 to 0.1875
Outputs:
- stream: bfloat16 [24576, 2048], P('sp', 'tp')
All inputs are finite; a program needn't handle non-finite values.
Results may differ from a plain program's by a relative error of at most 0.015.
Values may be sent and summed in bfloat16 or wider, within the bound.
No kernel may reach another device: no remote copies, remote signals or barrier semaphores. Data moves between devices by JAX's collectives and lax.ppermute only.
A program may use at most 64 MiB of HBM per device.

v0:
```python
import jax
import jax.numpy as jnp
from jax import lax
from jax.sharding import Mesh
from jax.sharding import PartitionSpec as P

SP = ("sp_0", "sp_1", "sp_2")


norm_floor = 0.01


def sent_to_all(array, axis):
    copies = jnp.broadcast_to(array, (lax.axis_size(axis), *array.shape))
    return lax.all_to_all(copies, axis, split_axis=0, concat_axis=0, tiled=True)


def laid_out(tiles, dim):
    dims = list(tiles.shape[1:])
    dims[dim] *= tiles.shape[0]
    return jnp.moveaxis(tiles, 0, dim).reshape(dims)


def gather_directly(array, axis, dim):
    tiles = sent_to_all(array, axis)
    return laid_out(tiles, dim)


def side_by_side(arrays, axis, dim, along):
    widths = [a.shape[along] for a in arrays]
    both = jnp.concatenate(arrays, axis=along)
    filled = lax.all_gather(both, axis, axis=dim, tiled=True)
    return tuple(jnp.split(filled, [sum(widths[:k]) for k in range(1, len(widths))], axis=along))


def with_halo(array, sides, width):
    for axis, dim in sides:
        size, length = (lax.axis_size(axis), array.shape[dim])
        up = [(i, (i + 1) % size) for i in range(size - 1)]
        down = [(j, i) for i, j in up]
        last = lax.slice_in_dim(array, length - width, length, axis=dim)
        first = lax.slice_in_dim(array, 0, width, axis=dim)
        before = lax.ppermute(last, axis, up)
        after = lax.ppermute(first, axis, down)
        array = jnp.concatenate([before, array, after], axis=dim)
    return array


def of_everyone(array, axis):
    everything = sent_to_all(array, axis)
    return jnp.sum(everything, axis=0)


def packed_total(arrays, axis):
    ends = [0]
    for a in arrays:
        ends.append(ends[-1] + a.size)
    total = of_everyone(jnp.concatenate([a.ravel() for a in arrays]), axis)
    return tuple((total[b:e].reshape(a.shape) for a, b, e in zip(arrays, ends, ends[1:])))


def stacked_from(array, axes, turns):
    tiles = array
    for k in turns:
        tiles = lax.all_gather(tiles, axes[k])
    done = turns[::-1]
    back = [done.index(k) for k in range(len(axes))]
    tiles = tiles.transpose(*back, *range(len(axes), tiles.ndim))
    return tiles.reshape(-1, *array.shape)


def gather_axes(array, axes, turns, dim):
    return laid_out(stacked_from(array, axes, turns), dim)


def split_up(array, dim, size):
    before, after = (array.shape[:dim], array.shape[dim + 1 :])
    return jnp.moveaxis(array.reshape(*before, size, -1, *after), dim, 0)


def sum_at_owner(array, axis, dim):
    tiles = split_up(array, dim, lax.axis_size(axis))
    arrived = lax.all_to_all(tiles, axis, split_axis=0, concat_axis=0, tiled=True)
    return arrived.astype(jnp.float32).sum(axis=0)


def body(tokens, norm_gain, w_value, w_gate, conv_taps, conv_bias, ln_gain, ln_shift, w_out):
    stream = tokens
    layer_count = w_value.shape[0]
    reach = conv_taps.shape[1] // 2
    local_channels = w_value.shape[2]
    channels = local_channels * lax.axis_size("tp")
    tok_rows = tokens.shape[0]
    for layer_index in range(layer_count):
        whole_rows = gather_directly(stream, "tp", 1)
        rows_f32 = whole_rows.astype(jnp.float32)
        scale_rows = lax.rsqrt(jnp.mean(rows_f32 * rows_f32, axis=-1, keepdims=True) + norm_floor)
        normed = (rows_f32 * scale_rows * norm_gain[layer_index]).astype(jnp.bfloat16)
        pieces = side_by_side((w_value[layer_index], w_gate[layer_index]), SP, 0, 1)
        value_rows = jnp.dot(normed, pieces[0], preferred_element_type=jnp.float32)
        gate_rows = jnp.dot(normed, pieces[1], preferred_element_type=jnp.float32)
        gated_input = (value_rows * jax.nn.sigmoid(gate_rows)).astype(jnp.bfloat16)
        padded = with_halo(gated_input, ((SP, 0),), reach)
        padded = padded.astype(jnp.float32)
        convolved = jnp.zeros((tok_rows, local_channels), jnp.float32) + conv_bias[layer_index]
        for offset in range(2 * reach + 1):
            convolved = (
                convolved + conv_taps[layer_index, offset] * padded[offset : offset + tok_rows]
            )
        moments = packed_total(
            (
                jnp.sum(convolved, axis=-1, keepdims=True),
                jnp.sum(convolved * convolved, axis=-1, keepdims=True),
            ),
            "tp",
        )
        average = moments[0] / channels
        spread = moments[1] / channels - average * average
        activated = jax.nn.silu(
            (convolved - average) * lax.rsqrt(spread + norm_floor) * ln_gain[layer_index]
            + ln_shift[layer_index]
        ).astype(jnp.bfloat16)
        partial_rows = jnp.dot(
            activated,
            gather_axes(w_out[layer_index], SP, (1, 0, 2), 1),
            preferred_element_type=jnp.float32,
        )
        summed = sum_at_owner(partial_rows.astype(jnp.bfloat16), "tp", 1)
        stream = (stream.astype(jnp.float32) + summed).astype(jnp.bfloat16)
    return stream


def solution(mesh):
    torus = Mesh(mesh.devices.reshape(8, 4, 2, mesh.shape["tp"]), ("sp_0", "sp_1", "sp_2", "tp"))
    return jax.shard_map(
        body,
        mesh=torus,
        in_specs=(
            P(SP, "tp"),
            P(),
            P(None, SP, "tp"),
            P(None, SP, "tp"),
            P(None, None, "tp"),
            P(None, "tp"),
            P(None, "tp"),
            P(None, "tp"),
            P(None, "tp", SP),
        ),
        out_specs=P(SP, "tp"),
        check_vma=False,
    )
```

profile of v0, /device:TPU:120, one launch (start us, length us, event | category | flops | bytes accessed | tf_op | source)
XLA Modules:
  0.0 330.5 jit_solution(233067519409634655)
XLA Ops:
  6.5 1.5 slice_bitcast_fusion
  8.7 1.4 fusion.149
  10.0 11.8 %all_gather.55 = bf16[4,256,32]{1,2,0:T(8,128)(2,1)S(1)} all-gather(bf16[1,256,32]{1,2,0:T(8,128)(2,1)S(1)} %get-tuple-element.119), channel_id=1, replica_groups=mesh['sp_0'=8,'sp_1'=4,'sp_2'=2,'tp'=4] {'sp_1'}, dimensions={0}, use_global_device_ids=true | all-gather | bytes 81920 | tf_op jit(solution)/shard_map/all_gather | solution.py:65
  21.9 28.6 %all-gather = bf16[32,256,32]{1,2,0:T(8,128)(2,1)} all-gather(bf16[4,256,32]{1,2,0:T(8,128)(2,1)S(1)} %all_gather.55), channel_id=2, replica_groups=mesh['sp_0'=8,'sp_1'=4,'sp_2'=2,'tp'=4] {'sp_0'}, dimensions={0}, use_global_device_ids=true | all-gather | bytes 589824 | tf_op jit(solution)/shard_map/all_gather | solution.py:65
  50.7 1.3 broadcast_in_dim.21
  52.0 4.4 %all-to-all-start = ((bf16[4,384,512]{1,2,0:T(8,128)(2,1)}), bf16[4,384,512]{1,2,0:T(8,128)(2,1)S(1)}, u32[]{:S(2)}, u32[]{:S(2)}) async-start(bf16[4,384,512]{1,2,0:T(8,128)(2,1)} %broadcast_in_dim.21), calls=%async_computation | async-start | bytes 3145728 | tf_op jit(solution)/shard_map/all_to_all | solution.py:15
  57.8 1.7 fusion.148
  59.5 1.6 fusion.147
  61.7 8.4 %all-to-all-done = bf16[4,384,512]{1,2,0:T(8,128)(2,1)S(1)} async-done(((bf16[4,384,512]{1,2,0:T(8,128)(2,1)}), bf16[4,384,512]{1,2,0:T(8,128)(2,1)S(1)}, u32[]{:S(2)}, u32[]{:S(2)}) %all-to-all-start) | async-done | bytes 1572896 | tf_op jit(solution)/shard_map/all_to_all | solution.py:15
  71.3 16.5 %all-gather.13.cloned.1.call-done = bf16[2048,512]{1,0:T(8,128)(2,1)} async-done(((bf16[32,512]{1,0:T(8,128)(2,1)}), bf16[2048,512]{1,0:T(8,128)(2,1)}) %all-gather.13.cloned.1.call-update) | async-done | bytes 2097168 | tf_op jit(solution)/shard_map/all_gather | solution.py:32
  87.7 2.0 fusion.10
  90.7 2.1 collective-permute-start
  92.9 3.4 %collective-permute-start.1 = (bf16[15,256]{1,0:T(8,128)(2,1)S(1)}, bf16[15,256]{1,0:T(8,128)(2,1)S(1)}, u32[]{:S(2)}, u32[]{:S(2)}) collective-permute-start(bf16[15,256]{1,0:T(8,128)(2,1)S(1)} %get-tuple-element.19), channel_id=1, source_target_pairs={{4,0},{8,4},{12,8},{16,12},{20,16},{24,20},{28,24},{32,28},{36,32}... | collective-permute-start | bytes 23048 | tf_op jit(solution)/shard_map/ppermute | solution.py:44
  98.0 1.7 fusion.137
  100.3 4.2 %all-to-all-start.1 = ((f32[4,1,768]{2,1,0:T(1,128)}), f32[4,1,768]{2,1,0:T(1,128)S(1)}, u32[]{:S(2)}, u32[]{:S(2)}) async-start(f32[4,1,768]{2,1,0:T(1,128)} %broadcast_in_dim.22), calls=%async_computation.1 | async-start | bytes 24576 | tf_op jit(solution)/shard_map/all_to_all | solution.py:15
  105.1 1.3 copy.39
  106.4 3.4 %all-to-all-done.1 = f32[4,1,768]{2,1,0:T(1,128)S(1)} async-done(((f32[4,1,768]{2,1,0:T(1,128)}), f32[4,1,768]{2,1,0:T(1,128)S(1)}, u32[]{:S(2)}, u32[]{:S(2)}) %all-to-all-start.1) | async-done | bytes 12320 | tf_op jit(solution)/shard_map/all_to_all | solution.py:15
  111.8 3.7 %all-to-all-start.2 = ((bf16[4,384,512]{2,1,0:T(8,128)(2,1)}), bf16[4,384,512]{2,1,0:T(8,128)(2,1)S(1)}, u32[]{:S(2)}, u32[]{:S(2)}) async-start(bf16[4,384,512]{2,1,0:T(8,128)(2,1)} %bitcast.197), calls=%async_computation.2 | async-start | bytes 3145728 | tf_op jit(solution)/shard_map/all_to_all | solution.py:83
  115.6 11.9 %all_gather.61 = bf16[4,256,32]{1,2,0:T(8,128)(2,1)S(1)} all-gather(bf16[1,256,32]{1,2,0:T(8,128)(2,1)S(1)} %copy-done.4), channel_id=1, replica_groups=mesh['sp_0'=8,'sp_1'=4,'sp_2'=2,'tp'=4] {'sp_1'}, dimensions={0}, use_global_device_ids=true | all-gather | bytes 81920 | tf_op jit(solution)/shard_map/all_gather | solution.py:65
  127.5 27.6 %all-gather.2 = bf16[32,256,32]{1,2,0:T(8,128)(2,1)} all-gather(bf16[4,256,32]{1,2,0:T(8,128)(2,1)S(1)} %all_gather.61), channel_id=4, replica_groups=mesh['sp_0'=8,'sp_1'=4,'sp_2'=2,'tp'=4] {'sp_0'}, dimensions={0}, use_global_device_ids=true | all-gather | bytes 589824 | tf_op jit(solution)/shard_map/all_gather | solution.py:65
  155.7 1.3 broadcast_in_dim.23
  157.0 4.9 %all-to-all-start.3 = ((bf16[4,384,512]{1,2,0:T(8,128)(2,1)}), bf16[4,384,512]{1,2,0:T(8,128)(2,1)S(1)}, u32[]{:S(2)}, u32[]{:S(2)}) async-start(bf16[4,384,512]{1,2,0:T(8,128)(2,1)} %broadcast_in_dim.23), calls=%async_computation.3 | async-start | bytes 3145728 | tf_op jit(solution)/shard_map/all_to_all | solution.py:15
  162.6 1.5 fusion.146
  164.1 14.6 %all-to-all-done.3 = bf16[4,384,512]{1,2,0:T(8,128)(2,1)S(1)} async-done(((bf16[4,384,512]{1,2,0:T(8,128)(2,1)}), bf16[4,384,512]{1,2,0:T(8,128)(2,1)S(1)}, u32[]{:S(2)}, u32[]{:S(2)}) %all-to-all-start.3) | async-done | bytes 1572896 | tf_op jit(solution)/shard_map/all_to_all | solution.py:15
  179.2 1.6 fusion.3
  180.8 2.1 all-gather.15.cloned.1.call-done
  182.9 2.5 fusion.12
  186.1 2.1 collective-permute-start.2
  188.3 3.6 %collective-permute-start.3 = (bf16[15,256]{1,0:T(8,128)(2,1)S(1)}, bf16[15,256]{1,0:T(8,128)(2,1)S(1)}, u32[]{:S(2)}, u32[]{:S(2)}) collective-permute-start(bf16[15,256]{1,0:T(8,128)(2,1)S(1)} %get-tuple-element.17), channel_id=1, source_target_pairs={{4,0},{8,4},{12,8},{16,12},{20,16},{24,20},{28,24},{32,28},{36,32}... | collective-permute-start | bytes 23048 | tf_op jit(solution)/shard_map/ppermute | solution.py:44
  191.9 1.8 fusion.145
  193.8 1.7 fusion.136
  196.1 4.2 %all-to-all-start.4 = ((f32[4,1,768]{2,1,0:T(1,128)}), f32[4,1,768]{2,1,0:T(1,128)S(1)}, u32[]{:S(2)}, u32[]{:S(2)}) async-start(f32[4,1,768]{2,1,0:T(1,128)} %broadcast_in_dim.24), calls=%async_computation.4 | async-start | bytes 24576 | tf_op jit(solution)/shard_map/all_to_all | solution.py:15
  200.4 1.3 copy.43
  201.7 4.0 %all-to-all-done.4 = f32[4,1,768]{2,1,0:T(1,128)S(1)} async-done(((f32[4,1,768]{2,1,0:T(1,128)}), f32[4,1,768]{2,1,0:T(1,128)S(1)}, u32[]{:S(2)}, u32[]{:S(2)}) %all-to-all-start.4) | async-done | bytes 12320 | tf_op jit(solution)/shard_map/all_to_all | solution.py:15
  206.6 22.5 %all_to_all.48 = bf16[4,384,512]{2,1,0:T(8,128)(2,1)S(1)} all-to-all(bf16[4,384,512]{2,1,0:T(8,128)(2,1)S(1)} %bitcast.198), channel_id=1, replica_groups=mesh['sp_0'=8,'sp_1'=4,'sp_2'=2,'tp'=4] {'tp'}, dimensions={0} | all-to-all | bytes 3145728 | tf_op jit(solution)/shard_map/all_to_all | solution.py:83
  229.7 1.3 broadcast_in_dim.25
  230.9 3.6 %all-to-all-start.6 = ((bf16[4,384,512]{1,2,0:T(8,128)(2,1)}), bf16[4,384,512]{1,2,0:T(8,128)(2,1)S(1)}, u32[]{:S(2)}, u32[]{:S(2)}) async-start(bf16[4,384,512]{1,2,0:T(8,128)(2,1)} %broadcast_in_dim.25), calls=%async_computation.6 | async-start | bytes 3145728 | tf_op jit(solution)/shard_map/all_to_all | solution.py:15
  234.6 11.9 %all_gather.67 = bf16[4,256,32]{1,2,0:T(8,128)(2,1)S(1)} all-gather(bf16[1,256,32]{1,2,0:T(8,128)(2,1)S(1)} %get-tuple-element.120), channel_id=1, replica_groups=mesh['sp_0'=8,'sp_1'=4,'sp_2'=2,'tp'=4] {'sp_1'}, dimensions={0}, use_global_device_ids=true | all-gather | bytes 81920 | tf_op jit(solution)/shard_map/all_gather | solution.py:65
  246.4 27.7 %all-gather.4 = bf16[32,256,32]{1,2,0:T(8,128)(2,1)} all-gather(bf16[4,256,32]{1,2,0:T(8,128)(2,1)S(1)} %all_gather.67), channel_id=6, replica_groups=mesh['sp_0'=8,'sp_1'=4,'sp_2'=2,'tp'=4] {'sp_0'}, dimensions={0}, use_global_device_ids=true | all-gather | bytes 589824 | tf_op jit(solution)/shard_map/all_gather | solution.py:65
  275.7 2.4 all-gather.17.cloned.1.call-done
  278.0 2.0 fusion.14
  280.8 2.1 collective-permute-start.4
  283.0 3.4 %collective-permute-start.5 = (bf16[15,256]{1,0:T(8,128)(2,1)S(1)}, bf16[15,256]{1,0:T(8,128)(2,1)S(1)}, u32[]{:S(2)}, u32[]{:S(2)}) collective-permute-start(bf16[15,256]{1,0:T(8,128)(2,1)S(1)} %get-tuple-element.15), channel_id=1, source_target_pairs={{4,0},{8,4},{12,8},{16,12},{20,16},{24,20},{28,24},{32,28},{36,32}... | collective-permute-start | bytes 23048 | tf_op jit(solution)/shard_map/ppermute | solution.py:44
  287.9 1.7 fusion.135
  290.2 4.1 %all-to-all-start.7 = ((f32[4,1,768]{2,1,0:T(1,128)}), f32[4,1,768]{2,1,0:T(1,128)S(1)}, u32[]{:S(2)}, u32[]{:S(2)}) async-start(f32[4,1,768]{2,1,0:T(1,128)} %broadcast_in_dim.26), calls=%async_computation.7 | async-start | bytes 24576 | tf_op jit(solution)/shard_map/all_to_all | solution.py:15
  294.4 1.3 copy.47
  295.7 4.0 %all-to-all-done.7 = f32[4,1,768]{2,1,0:T(1,128)S(1)} async-done(((f32[4,1,768]{2,1,0:T(1,128)}), f32[4,1,768]{2,1,0:T(1,128)S(1)}, u32[]{:S(2)}, u32[]{:S(2)}) %all-to-all-start.7) | async-done | bytes 12320 | tf_op jit(solution)/shard_map/all_to_all | solution.py:15
  300.6 21.9 %all_to_all.49 = bf16[4,384,512]{2,1,0:T(8,128)(2,1)S(1)} all-to-all(bf16[4,384,512]{2,1,0:T(8,128)(2,1)S(1)} %bitcast.199), channel_id=1, replica_groups=mesh['sp_0'=8,'sp_1'=4,'sp_2'=2,'tp'=4] {'tp'}, dimensions={0} | all-to-all | bytes 3145728 | tf_op jit(solution)/shard_map/all_to_all | solution.py:83
  (207 shorter events, 20.0 us)
Async XLA Ops:
  6.5 43.9 %copy-start = (bf16[384,512]{1,0:T(8,128)(2,1)S(1)}, bf16[384,512]{1,0:T(8,128)(2,1)}, u32[]{:S(2)}) copy-start(bf16[384,512]{1,0:T(8,128)(2,1)} %param.9) | copy-start | bytes 1179652
  6.5 81.2 %all-gather.13.cloned.1.call-start = ((), (), s32[]{:S(2)}) async-start(), calls=%async_computation.9 | async-start | bytes 2129920 | tf_op jit(solution)/shard_map/all_gather | solution.py:32
  8.6 96.5 %all-gather.19.cloned.1.call-start = ((), (), s32[]{:S(2)}) async-start(), calls=%async_computation.12 | async-start | bytes 1572864 | tf_op jit(solution)/shard_map/all_gather | solution.py:65
  52.0 9.1 %copy-start.7 = (f32[3,2048]{1,0:T(4,128)S(1)}, f32[3,2048]{1,0:T(4,128)}, u32[]{:S(2)}) copy-start(f32[3,2048]{1,0:T(4,128)} %param.10) | copy-start | bytes 73732
  52.0 18.1 %all-to-all-start = ((bf16[4,384,512]{1,2,0:T(8,128)(2,1)}), bf16[4,384,512]{1,2,0:T(8,128)(2,1)S(1)}, u32[]{:S(2)}, u32[]{:S(2)}) async-start(bf16[4,384,512]{1,2,0:T(8,128)(2,1)} %broadcast_in_dim.21), calls=%async_computation | async-start | bytes 3145728 | tf_op jit(solution)/shard_map/all_to_all | solution.py:15
  56.5 126.5 %all-gather.15.cloned.1.call-start = ((), (), s32[]{:S(2)}) async-start(), calls=%async_computation.10 | async-start | bytes 2129920 | tf_op jit(solution)/shard_map/all_gather | solution.py:32
  89.8 7.9 %copy-start.24 = (f32[1,1,256]{2,1,0:T(1,128)S(1)}, f32[1,1,256]{2,1,0:T(1,128)}, u32[]{:S(2)}) copy-start(f32[1,1,256]{2,1,0:T(1,128)} %get-tuple-element.96) | copy-start | bytes 3076
  89.8 7.9 %copy-start.25 = (f32[1,1,256]{2,1,0:T(1,128)S(1)}, f32[1,1,256]{2,1,0:T(1,128)}, u32[]{:S(2)}) copy-start(f32[1,1,256]{2,1,0:T(1,128)} %get-tuple-element.97) | copy-start | bytes 3076
  89.8 7.9 %copy-start.26 = (f32[1,1,256]{2,1,0:T(1,128)S(1)}, f32[1,1,256]{2,1,0:T(1,128)}, u32[]{:S(2)}) copy-start(f32[1,1,256]{2,1,0:T(1,128)} %get-tuple-element.98) | copy-start | bytes 3076
  89.8 7.9 %copy-start.27 = (f32[1,1,256]{2,1,0:T(1,128)S(1)}, f32[1,1,256]{2,1,0:T(1,128)}, u32[]{:S(2)}) copy-start(f32[1,1,256]{2,1,0:T(1,128)} %get-tuple-element.99) | copy-start | bytes 3076
  89.8 7.9 %copy-start.28 = (f32[1,1,256]{2,1,0:T(1,128)S(1)}, f32[1,1,256]{2,1,0:T(1,128)}, u32[]{:S(2)}) copy-start(f32[1,1,256]{2,1,0:T(1,128)} %get-tuple-element.100) | copy-start | bytes 3076
  89.8 7.9 %copy-start.29 = (f32[1,1,256]{2,1,0:T(1,128)S(1)}, f32[1,1,256]{2,1,0:T(1,128)}, u32[]{:S(2)}) copy-start(f32[1,1,256]{2,1,0:T(1,128)} %get-tuple-element.101) | copy-start | bytes 3076
  89.8 7.9 %copy-start.30 = (f32[1,1,256]{2,1,0:T(1,128)S(1)}, f32[1,1,256]{2,1,0:T(1,128)}, u32[]{:S(2)}) copy-start(f32[1,1,256]{2,1,0:T(1,128)} %get-tuple-element.102) | copy-start | bytes 3076
  89.8 7.9 %copy-start.31 = (f32[1,1,256]{2,1,0:T(1,128)S(1)}, f32[1,1,256]{2,1,0:T(1,128)}, u32[]{:S(2)}) copy-start(f32[1,1,256]{2,1,0:T(1,128)} %get-tuple-element.103) | copy-start | bytes 3076
  89.8 7.9 %copy-start.32 = (f32[1,1,256]{2,1,0:T(1,128)S(1)}, f32[1,1,256]{2,1,0:T(1,128)}, u32[]{:S(2)}) copy-start(f32[1,1,256]{2,1,0:T(1,128)} %get-tuple-element.104) | copy-start | bytes 3076
  89.8 7.9 %copy-start.33 = (f32[1,1,256]{2,1,0:T(1,128)S(1)}, f32[1,1,256]{2,1,0:T(1,128)}, u32[]{:S(2)}) copy-start(f32[1,1,256]{2,1,0:T(1,128)} %get-tuple-element.105) | copy-start | bytes 3076
  89.9 7.9 %copy-start.34 = (f32[1,1,256]{2,1,0:T(1,128)S(1)}, f32[1,1,256]{2,1,0:T(1,128)}, u32[]{:S(2)}) copy-start(f32[1,1,256]{2,1,0:T(1,128)} %get-tuple-element.106) | copy-start | bytes 3076
  89.9 7.9 %copy-start.35 = (f32[1,1,256]{2,1,0:T(1,128)S(1)}, f32[1,1,256]{2,1,0:T(1,128)}, u32[]{:S(2)}) copy-start(f32[1,1,256]{2,1,0:T(1,128)} %get-tuple-element.107) | copy-start | bytes 3076
  89.9 7.9 %copy-start.36 = (f32[1,1,256]{2,1,0:T(1,128)S(1)}, f32[1,1,256]{2,1,0:T(1,128)}, u32[]{:S(2)}) copy-start(f32[1,1,256]{2,1,0:T(1,128)} %get-tuple-element.108) | copy-start | bytes 3076
  89.9 7.9 %copy-start.37 = (f32[1,1,256]{2,1,0:T(1,128)S(1)}, f32[1,1,256]{2,1,0:T(1,128)}, u32[]{:S(2)}) copy-start(f32[1,1,256]{2,1,0:T(1,128)} %get-tuple-element.109) | copy-start | bytes 3076
  89.9 7.9 %copy-start.38 = (f32[1,1,256]{2,1,0:T(1,128)S(1)}, f32[1,1,256]{2,1,0:T(1,128)}, u32[]{:S(2)}) copy-start(f32[1,1,256]{2,1,0:T(1,128)} %get-tuple-element.110) | copy-start | bytes 3076
  89.9 7.9 %copy-start.39 = (f32[1,1,256]{2,1,0:T(1,128)S(1)}, f32[1,1,256]{2,1,0:T(1,128)}, u32[]{:S(2)}) copy-start(f32[1,1,256]{2,1,0:T(1,128)} %get-tuple-element.111) | copy-start | bytes 3076
  89.9 7.9 %copy-start.40 = (f32[1,1,256]{2,1,0:T(1,128)S(1)}, f32[1,1,256]{2,1,0:T(1,128)}, u32[]{:S(2)}) copy-start(f32[1,1,256]{2,1,0:T(1,128)} %get-tuple-element.112) | copy-start | bytes 3076
  89.9 7.9 %copy-start.41 = (f32[1,1,256]{2,1,0:T(1,128)S(1)}, f32[1,1,256]{2,1,0:T(1,128)}, u32[]{:S(2)}) copy-start(f32[1,1,256]{2,1,0:T(1,128)} %get-tuple-element.82) | copy-start | bytes 3076
  89.9 7.9 %copy-start.42 = (f32[1,1,256]{2,1,0:T(1,128)S(1)}, f32[1,1,256]{2,1,0:T(1,128)}, u32[]{:S(2)}) copy-start(f32[1,1,256]{2,1,0:T(1,128)} %get-tuple-element.83) | copy-start | bytes 3076
  90.7 6.2 %collective-permute-start = (bf16[15,256]{1,0:T(8,128)(2,1)S(1)}, bf16[15,256]{1,0:T(8,128)(2,1)S(1)}, u32[]{:S(2)}, u32[]{:S(2)}) collective-permute-start(bf16[15,256]{1,0:T(8,128)(2,1)S(1)} %get-tuple-element.18), channel_id=1, source_target_pairs={{0,4},{4,8},{8,12},{12,16},{16,20},{20,24},{24,28},{28,32},{32,36}... | collective-permute-start | bytes 23048 | tf_op jit(solution)/shard_map/ppermute | solution.py:43
  92.9 4.8 %collective-permute-start.1 = (bf16[15,256]{1,0:T(8,128)(2,1)S(1)}, bf16[15,256]{1,0:T(8,128)(2,1)S(1)}, u32[]{:S(2)}, u32[]{:S(2)}) collective-permute-start(bf16[15,256]{1,0:T(8,128)(2,1)S(1)} %get-tuple-element.19), channel_id=1, source_target_pairs={{4,0},{8,4},{12,8},{16,12},{20,16},{24,20},{28,24},{32,28},{36,32}... | collective-permute-start | bytes 23048 | tf_op jit(solution)/shard_map/ppermute | solution.py:44
  100.3 9.5 %all-to-all-start.1 = ((f32[4,1,768]{2,1,0:T(1,128)}), f32[4,1,768]{2,1,0:T(1,128)S(1)}, u32[]{:S(2)}, u32[]{:S(2)}) async-start(f32[4,1,768]{2,1,0:T(1,128)} %broadcast_in_dim.22), calls=%async_computation.1 | async-start | bytes 24576 | tf_op jit(solution)/shard_map/all_to_all | solution.py:15
  111.8 43.3 %all-to-all-start.2 = ((bf16[4,384,512]{2,1,0:T(8,128)(2,1)}), bf16[4,384,512]{2,1,0:T(8,128)(2,1)S(1)}, u32[]{:S(2)}, u32[]{:S(2)}) async-start(bf16[4,384,512]{2,1,0:T(8,128)(2,1)} %bitcast.197), calls=%async_computation.2 | async-start | bytes 3145728 | tf_op jit(solution)/shard_map/all_to_all | solution.py:83
  115.5 84.8 %all-gather.21.cloned.1.call-start = ((), (), s32[]{:S(2)}) async-start(), calls=%async_computation.13 | async-start | bytes 1572864 | tf_op jit(solution)/shard_map/all_gather | solution.py:65
  157.0 21.7 %all-to-all-start.3 = ((bf16[4,384,512]{1,2,0:T(8,128)(2,1)}), bf16[4,384,512]{1,2,0:T(8,128)(2,1)S(1)}, u32[]{:S(2)}, u32[]{:S(2)}) async-start(bf16[4,384,512]{1,2,0:T(8,128)(2,1)} %broadcast_in_dim.23), calls=%async_computation.3 | async-start | bytes 3145728 | tf_op jit(solution)/shard_map/all_to_all | solution.py:15
  161.9 17.3 %copy-start.5 = (f32[1,2048]{1,0:T(1,128)S(1)}, f32[1,2048]{1,0:T(1,128)}, u32[]{:S(2)}) copy-start(f32[1,2048]{1,0:T(1,128)} %get-tuple-element.124) | copy-start | bytes 24580
  161.9 116.1 %all-gather.17.cloned.1.call-start = ((), (), s32[]{:S(2)}) async-start(), calls=%async_computation.11 | async-start | bytes 2129920 | tf_op jit(solution)/shard_map/all_gather | solution.py:32
  185.4 8.3 %copy-start.9 = (f32[1,1,256]{2,1,0:T(1,128)S(1)}, f32[1,1,256]{2,1,0:T(1,128)}, u32[]{:S(2)}) copy-start(f32[1,1,256]{2,1,0:T(1,128)} %get-tuple-element.78) | copy-start | bytes 3076
  185.5 8.3 %copy-start.10 = (f32[1,1,256]{2,1,0:T(1,128)S(1)}, f32[1,1,256]{2,1,0:T(1,128)}, u32[]{:S(2)}) copy-start(f32[1,1,256]{2,1,0:T(1,128)} %get-tuple-element.79) | copy-start | bytes 3076
  185.5 8.3 %copy-start.11 = (f32[1,1,256]{2,1,0:T(1,128)S(1)}, f32[1,1,256]{2,1,0:T(1,128)}, u32[]{:S(2)}) copy-start(f32[1,1,256]{2,1,0:T(1,128)} %get-tuple-element.80) | copy-start | bytes 3076
  185.5 8.3 %copy-start.12 = (f32[1,1,256]{2,1,0:T(1,128)S(1)}, f32[1,1,256]{2,1,0:T(1,128)}, u32[]{:S(2)}) copy-start(f32[1,1,256]{2,1,0:T(1,128)} %get-tuple-element.81) | copy-start | bytes 3076
  185.5 8.3 %copy-start.56 = (f32[1,256]{1,0:T(1,128)S(1)}, f32[1,256]{1,0:T(1,128)}, u32[]{:S(2)}) copy-start(f32[1,256]{1,0:T(1,128)} %get-tuple-element.135) | copy-start | bytes 3076
  186.1 7.6 %collective-permute-start.2 = (bf16[15,256]{1,0:T(8,128)(2,1)S(1)}, bf16[15,256]{1,0:T(8,128)(2,1)S(1)}, u32[]{:S(2)}, u32[]{:S(2)}) collective-permute-start(bf16[15,256]{1,0:T(8,128)(2,1)S(1)} %get-tuple-element.16), channel_id=1, source_target_pairs={{0,4},{4,8},{8,12},{12,16},{16,20},{20,24},{24,28},{28,32},{32,36}... | collective-permute-start | bytes 23048 | tf_op jit(solution)/shard_map/ppermute | solution.py:43
  188.3 5.4 %collective-permute-start.3 = (bf16[15,256]{1,0:T(8,128)(2,1)S(1)}, bf16[15,256]{1,0:T(8,128)(2,1)S(1)}, u32[]{:S(2)}, u32[]{:S(2)}) collective-permute-start(bf16[15,256]{1,0:T(8,128)(2,1)S(1)} %get-tuple-element.17), channel_id=1, source_target_pairs={{4,0},{8,4},{12,8},{16,12},{20,16},{24,20},{28,24},{32,28},{36,32}... | collective-permute-start | bytes 23048 | tf_op jit(solution)/shard_map/ppermute | solution.py:44
  196.1 9.6 %all-to-all-start.4 = ((f32[4,1,768]{2,1,0:T(1,128)}), f32[4,1,768]{2,1,0:T(1,128)S(1)}, u32[]{:S(2)}, u32[]{:S(2)}) async-start(f32[4,1,768]{2,1,0:T(1,128)} %broadcast_in_dim.24), calls=%async_computation.4 | async-start | bytes 24576 | tf_op jit(solution)/shard_map/all_to_all | solution.py:15
  230.9 43.2 %all-to-all-start.6 = ((bf16[4,384,512]{1,2,0:T(8,128)(2,1)}), bf16[4,384,512]{1,2,0:T(8,128)(2,1)S(1)}, u32[]{:S(2)}, u32[]{:S(2)}) async-start(bf16[4,384,512]{1,2,0:T(8,128)(2,1)} %broadcast_in_dim.25), calls=%async_computation.6 | async-start | bytes 3145728 | tf_op jit(solution)/shard_map/all_to_all | solution.py:15
  234.5 59.8 %all-gather.23.cloned.1.call-start = ((), (), s32[]{:S(2)}) async-start(), calls=%async_computation.14 | async-start | bytes 1572864 | tf_op jit(solution)/shard_map/all_gather | solution.py:65
  280.8 6.6 %collective-permute-start.4 = (bf16[15,256]{1,0:T(8,128)(2,1)S(1)}, bf16[15,256]{1,0:T(8,128)(2,1)S(1)}, u32[]{:S(2)}, u32[]{:S(2)}) collective-permute-start(bf16[15,256]{1,0:T(8,128)(2,1)S(1)} %get-tuple-element.14), channel_id=1, source_target_pairs={{0,4},{4,8},{8,12},{12,16},{16,20},{20,24},{24,28},{28,32},{32,36}... | collective-permute-start | bytes 23048 | tf_op jit(solution)/shard_map/ppermute | solution.py:43
  283.0 4.8 %collective-permute-start.5 = (bf16[15,256]{1,0:T(8,128)(2,1)S(1)}, bf16[15,256]{1,0:T(8,128)(2,1)S(1)}, u32[]{:S(2)}, u32[]{:S(2)}) collective-permute-start(bf16[15,256]{1,0:T(8,128)(2,1)S(1)} %get-tuple-element.15), channel_id=1, source_target_pairs={{4,0},{8,4},{12,8},{16,12},{20,16},{24,20},{28,24},{32,28},{36,32}... | collective-permute-start | bytes 23048 | tf_op jit(solution)/shard_map/ppermute | solution.py:44
  289.6 10.1 %copy-start.61 = (f32[1,256]{1,0:T(1,128)S(1)}, f32[1,256]{1,0:T(1,128)}, u32[]{:S(2)}) copy-start(f32[1,256]{1,0:T(1,128)} %get-tuple-element.127) | copy-start | bytes 3076
  289.6 10.1 %copy-start.62 = (f32[1,256]{1,0:T(1,128)S(1)}, f32[1,256]{1,0:T(1,128)}, u32[]{:S(2)}) copy-start(f32[1,256]{1,0:T(1,128)} %get-tuple-element.130) | copy-start | bytes 3076
  290.2 9.5 %all-to-all-start.7 = ((f32[4,1,768]{2,1,0:T(1,128)}), f32[4,1,768]{2,1,0:T(1,128)S(1)}, u32[]{:S(2)}, u32[]{:S(2)}) async-start(f32[4,1,768]{2,1,0:T(1,128)} %broadcast_in_dim.26), calls=%async_computation.7 | async-start | bytes 24576 | tf_op jit(solution)/shard_map/all_to_all | solution.py:15
  (37 other events, 247.5 us)
Sparse Core Ops, SparseCore 0:
  10.1 77.5 all-gather.12
  89.5 13.4 all-gather.18
  105.8 77.1 all-gather.14
  184.6 13.4 all-gather.20
  200.8 77.2 all-gather.16
  279.7 13.8 all-gather.22
where the time goes:
time: 337 us; the launch traced here: 330 us
  blocking collectives  164 us (49%)
  waiting for transfers between devices  56.8 us (17%)
  starting transfers between devices  46.2 us (14%)
  local copies, waits for them, and re-layouts  25.3 us (8%)
  between operations  14.8 us (4%)
  other arithmetic  13.4 us (4%)
  matrix products  10.3 us (3%)
    all_gather x6, blocking collectives, stacked_from(): tiles = lax.all_gather(tiles, axes[k])  119 us
    all_to_all x2, blocking collectives, sum_at_owner(): lax.all_to_all(tiles, axis, split_axis=0, concat_axis=0, tiled=True)  44.4 us
    all_to_all x6, waiting for transfers between devices, sent_to_all(): return lax.all_to_all(copies, axis, split_axis=0, concat_axis=0, tiled=True)  34.5 us
    all_to_all x6, starting transfers between devices, sent_to_all(): return lax.all_to_all(copies, axis, split_axis=0, concat_axis=0, tiled=True)  25.5 us
    all_gather x3, waiting for transfers between devices, side_by_side(): filled = lax.all_gather(both, axis, axis=dim, tiled=True)  21 us
    ppermute x3, starting transfers between devices, with_halo(): after = lax.ppermute(first, axis, down)  10.5 us
    slice x5, local copies, waits for them, and re-layouts, body(): conv_taps[layer_index, offset] * padded[offset:offset + tok_rows]  7.65 us
  transfers between devices with their start and end apart: 19, of which 10 were waited for; matrix products, arithmetic and copies ran while one was open for 13% of the time, Pallas kernels for 0%

commit v1 on v0

v1 whole, which is shorter than its diff:
```python
import functools

import jax
import jax.numpy as jnp
from jax import lax
from jax.experimental import pallas as pl
from jax.experimental.pallas import tpu as pltpu
from jax.sharding import Mesh
from jax.sharding import PartitionSpec as P

SP = ("z", "y", "c")
EDGE = 16
LANES = 128
norm_floor = 0.01
bf16, f32 = jnp.bfloat16, jnp.float32


def to_all(array, axis):
    copies = jnp.broadcast_to(array, (lax.axis_size(axis), *array.shape))
    return lax.all_to_all(copies, axis, split_axis=0, concat_axis=0, tiled=True)


def core_swap(array):
    return lax.ppermute(array, "c", [(0, 1), (1, 0)])


def after(array, *others):
    return lax.optimization_barrier((array, *others))[0]


def place_rows(core, pieces, store):
    n_y, n_z, n_i, _ = pieces[0].shape

    def step(z, carry):
        for y in range(n_y):
            for piece, c in zip(pieces, (core, 1 - core)):
                row = pl.multiple_of(((z * n_y + y) * 2 + c) * n_i, n_i)
                store(pl.ds(row, n_i), piece[y, z])
        return carry

    lax.fori_loop(0, n_z, step, 0)


def up_kernel(layer, total, info, stream, gain, own, other, out, weights, normed):
    n_x, rows, width = stream.shape
    ch = out.shape[-1]

    def store(where, value):
        weights[where, :] = value

    place_rows(info[0], (own, other), store)
    squares = jnp.zeros((rows, 1), f32)
    for b in range(n_x):
        block = stream[b].astype(f32)
        squares += jnp.sum(block * block, axis=-1, keepdims=True)
    scale = lax.rsqrt(squares * (1.0 / (n_x * width)) + norm_floor)
    for b in range(n_x):
        lanes = slice(b * width, (b + 1) * width)
        block = stream[b].astype(f32)
        normed[:, lanes] = (block * scale * gain[layer : layer + 1, lanes]).astype(bf16)
    both = jnp.dot(normed[...], weights[...], preferred_element_type=f32)
    gated = both[:, :ch] * jax.nn.sigmoid(both[:, ch:])
    t = info[2 + layer] + lax.broadcasted_iota(jnp.int32, (rows, 1), 0)
    gated = jnp.where((t >= 0) & (t < total), gated, 0.0).astype(bf16)
    for b in range(out.shape[0]):
        out[b] = gated


def down_kernel(layer, last, info, gated, par, own, other, stream, out, weights, act, conv):
    n_x, rows, ch = gated.shape
    keep = rows - 2 * EDGE
    taps = par.shape[2] - 3
    shift = EDGE - taps // 2
    step_rows = 64 if keep % 64 == 0 else 32
    window = step_rows + 2 * EDGE
    strips = [(x, s) for x in range(n_x) for s in range(0, ch, LANES)]
    inverse = 1.0 / (n_x * ch)

    for x in range(n_x):

        def store(where, value, x=x):
            weights[where, x * ch : (x + 1) * ch] = value

        place_rows(info[0], (own.at[x], other.at[x]), store)

    def chunk(i, carry):
        first = pl.multiple_of(i * step_rows, step_rows)
        total = jnp.zeros((step_rows, LANES), f32)
        squares = jnp.zeros((step_rows, LANES), f32)
        for x, s in strips:
            lanes = slice(s, s + LANES)
            win = gated[x, pl.ds(first, window), lanes].astype(f32)
            acc = jnp.zeros((step_rows, LANES), f32) + par[x, layer, taps : taps + 1, lanes]
            for r in range(8):
                turned = pltpu.roll(win, window - r, 0) if r else win
                for q in range(window // 8):
                    k = 8 * q + r - shift
                    if 0 <= k < taps:
                        tap = par[x, layer, k : k + 1, lanes]
                        acc = acc + tap * turned[8 * q : 8 * q + step_rows]
            conv[:, x * ch + s : x * ch + s + LANES] = acc
            total = total + acc
            squares = squares + acc * acc
        average = jnp.sum(total, axis=-1, keepdims=True) * inverse
        spread = jnp.sum(squares, axis=-1, keepdims=True) * inverse - average * average
        scale = lax.rsqrt(spread + norm_floor)
        for x, s in strips:
            lanes = slice(s, s + LANES)
            wide = slice(x * ch + s, x * ch + s + LANES)
            value = (conv[:, wide] - average) * scale
            value = value * par[x, layer, taps + 1 : taps + 2, lanes] + par[x, layer, taps + 2 : taps + 3, lanes]
            act[pl.ds(first, step_rows), wide] = (value * jax.nn.sigmoid(value)).astype(bf16)
        return carry

    lax.fori_loop(0, keep // step_rows, chunk, 0)
    width = stream.shape[2]
    dims = (((1,), (1,)), ((), ()))
    if last:
        added = lax.dot_general(act[...], weights[...], dims, preferred_element_type=f32)
        base = stream[info[1], EDGE : EDGE + keep].astype(f32)
        out[...] = (base + added).astype(bf16)
    else:
        for b in range(n_x):
            part = weights[b * width : (b + 1) * width]
            added = lax.dot_general(act[...], part, dims, preferred_element_type=f32)
            out[b] = (stream[b, EDGE : EDGE + keep].astype(f32) + added).astype(bf16)


def in_vmem(count):
    return [pl.BlockSpec(memory_space=pltpu.SMEM)] + [pl.BlockSpec(memory_space=pltpu.VMEM)] * count


def up(layer, total, info, stream, gain, own, other):
    n_x, rows, width = stream.shape
    pair = own.shape[-1]
    return pl.pallas_call(
        functools.partial(up_kernel, layer, total),
        out_shape=jax.ShapeDtypeStruct((n_x, rows, pair // 2), bf16),
        in_specs=in_vmem(4),
        out_specs=pl.BlockSpec(memory_space=pltpu.VMEM),
        scratch_shapes=[
            pltpu.VMEM((n_x * width, pair), bf16),
            pltpu.VMEM((rows, n_x * width), bf16),
        ],
        name=f"up_{layer}",
    )(info, stream, gain, own, other)


def down(layer, last, info, gated, par, own, other, stream):
    n_x, rows, ch = gated.shape
    keep = rows - 2 * EDGE
    width = stream.shape[2]
    features = width if last else n_x * width
    step_rows = 64 if keep % 64 == 0 else 32
    shape = (keep, width) if last else (n_x, keep, width)
    return pl.pallas_call(
        functools.partial(down_kernel, layer, last),
        out_shape=jax.ShapeDtypeStruct(shape, bf16),
        in_specs=in_vmem(5),
        out_specs=pl.BlockSpec(memory_space=pltpu.VMEM),
        scratch_shapes=[
            pltpu.VMEM((features, n_x * ch), bf16),
            pltpu.VMEM((keep, n_x * ch), bf16),
            pltpu.VMEM((step_rows, n_x * ch), f32),
        ],
        name=f"down_{layer}",
    )(info, gated, par, own, other, stream)


def body(tokens, norm_gain, w_value, w_gate, conv_taps, conv_bias, ln_gain, ln_shift, w_out):
    layers, n_i, ch = w_value.shape
    n_x = lax.axis_size("x")
    n_tok, f_loc = tokens.shape
    halo = EDGE * layers
    size = lax.axis_size(SP)
    total = size * n_tok
    place = lax.axis_index(SP) * n_tok
    info = jnp.stack(
        [lax.axis_index("c"), lax.axis_index("x")] + [place - EDGE * (layers - l) for l in range(layers)]
    ).astype(jnp.int32)

    before = lax.ppermute(tokens[n_tok - halo :], SP, [(i, i + 1) for i in range(size - 1)])
    behind = lax.ppermute(tokens[:halo], SP, [(i + 1, i) for i in range(size - 1)])
    stream = to_all(jnp.concatenate([before, tokens, behind], axis=0), "x")

    par = jnp.concatenate([conv_taps, conv_bias[:, None], ln_gain[:, None], ln_shift[:, None]], axis=1)
    par = to_all(par, "x")

    out_t = jnp.swapaxes(w_out, 1, 2)
    ups, outs = [], []
    for l in range(layers):
        outward = to_all(to_all(out_t[l], "z"), "y")
        inward = to_all(to_all(jnp.concatenate([w_value[l], w_gate[l]], axis=1), "z"), "y")
        if l < layers - 1:
            outward = to_all(outward, "x")
        else:
            n_y, n_z = outward.shape[:2]
            by_x = jnp.moveaxis(outward.reshape(n_y, n_x, n_z // n_x, n_i, ch), 1, 0)
            outward = lax.all_to_all(by_x, "x", split_axis=0, concat_axis=0, tiled=True)
        ups.append((inward, core_swap(inward)))
        outs.append((outward, core_swap(outward)))

    for l in range(layers):
        gated = up(l, total, info, stream, norm_gain, *ups[l])
        gated = lax.all_to_all(gated, "x", split_axis=0, concat_axis=0, tiled=True)
        stream = down(l, l == layers - 1, info, gated, par, *outs[l], stream)
    return stream


def solution(mesh):
    torus = Mesh(mesh.devices.reshape(8, 4, 2, mesh.shape["tp"]), ("z", "y", "c", "x"))
    return jax.shard_map(
        body,
        mesh=torus,
        in_specs=(
            P(SP, "x"),
            P(),
            P(None, SP, "x"),
            P(None, SP, "x"),
            P(None, None, "x"),
            P(None, "x"),
            P(None, "x"),
            P(None, "x"),
            P(None, "x", SP),
        ),
        out_specs=P(SP, "x"),
        check_vma=False,
    )
```

time: 337 us -> 369 us (1.095); the launches traced: 330 us -> 367 us
  Pallas kernels: 0 us -> 51.7 us
  waiting for transfers between devices: 56.8 us -> 83.4 us
  starting transfers between devices: 46.2 us -> 61.9 us
  between operations: 14.8 us -> 0.23 us
  other arithmetic: 13.4 us -> 0.96 us
  local copies, waits for them, and re-layouts: 25.3 us -> 14 us
  matrix products: 10.3 us -> 0 us
  blocking collectives: 164 us -> 155 us
    all_gather x6 -> x0, blocking collectives: 119 us -> none  [stacked_from(): tiles = lax.all_gather(tiles, axes[k])]
    all_to_all x2 -> x9, blocking collectives: 44.4 us -> 155 us  [to_all(): return lax.all_to_all(copies, axis, split_axis=0, concat_axis=0, tiled=True)]
    pallas_call x0 -> x6, Pallas kernels: none -> 51.7 us  [the longest x3 37.6 us: down(): pl.pallas_call(functools.partial(down_kernel, layer, last), out_shape=jax...]
    all_to_all x7 -> x11, waiting for transfers between devices: 34.6 us -> 77.7 us  [the longest x7 45.3 us: to_all(): return lax.all_to_all(copies, axis, split_axis=0, concat_axis=0, tiled=True)]
    all_to_all x7 -> x11, starting transfers between devices: 29.2 us -> 54.9 us  [the longest x7 38.8 us: to_all(): return lax.all_to_all(copies, axis, split_axis=0, concat_axis=0, tiled=True)]
    all_gather x6 -> x0, waiting for transfers between devices: 21 us -> none  [the longest x3 21 us: side_by_side(): filled = lax.all_gather(both, axis, axis=dim, tiled=True)]
    slice x13 -> x1, local copies, waits for them, and re-layouts: 11.4 us -> 0.01 us  [body(): tokens[n_tok - halo:]]
    dot_general x9 -> x0, matrix products: 10.3 us -> none  [the longest x3 6.46 us: body(): gate_rows = jnp.dot(normed, pieces[1], preferred_element_type=jnp.float32)]
  transfers between devices with their start and end apart: 19 -> 19, of which waited for: 10 -> 13; matrix products, arithmetic and copies ran while one was open for 13% -> 2% of each run, Pallas kernels for 0% -> 12%
where the time goes in v1:
time: 369 us; the launch traced here: 367 us
  blocking collectives  155 us (42%)
  waiting for transfers between devices  83.4 us (23%)
  starting transfers between devices  61.9 us (17%)
  Pallas kernels  51.7 us (14%)
  local copies, waits for them, and re-layouts  14 us (4%)
    all_to_all x9, blocking collectives, to_all(): return lax.all_to_all(copies, axis, split_axis=0, concat_axis=0, tiled=True)  155 us
    all_to_all x7, waiting for transfers between devices, to_all(): return lax.all_to_all(copies, axis, split_axis=0, concat_axis=0, tiled=True)  45.3 us
    all_to_all x7, starting transfers between devices, to_all(): return lax.all_to_all(copies, axis, split_axis=0, concat_axis=0, tiled=True)  38.8 us
    pallas_call x3, Pallas kernels, down(): pl.pallas_call(functools.partial(down_kernel, layer, last), out_shape=jax...  37.6 us
    all_to_all x3, waiting for transfers between devices, body(): gated = lax.all_to_all(gated, 'x', split_axis=0, concat_axis=0, tiled=True)  32.5 us
    pallas_call x3, Pallas kernels, up(): pl.pallas_call(functools.partial(up_kernel, layer, total), out_shape=jax....  14.1 us
    all_to_all x3, starting transfers between devices, body(): gated = lax.all_to_all(gated, 'x', split_axis=0, concat_axis=0, tiled=True)  12.6 us
    broadcast_in_dim x16, local copies, waits for them, and re-layouts, to_all(): copies = jnp.broadcast_to(array, (lax.axis_size(axis), *array.shape))  7.74 us
  transfers between devices with their start and end apart: 19, of which 13 were waited for; matrix products, arithmetic and copies ran while one was open for 2% of the time, Pallas kernels for 12%

profile of v1, /device:TPU:120, one launch (start us, length us, event | category | flops | bytes accessed | tf_op | source)
XLA Modules:
  0.0 367.0 jit_solution(8056163000350020082)
XLA Ops:
  0.8 13.3 %all_to_all.100 = bf16[8,32,256]{2,1,0:T(8,128)(2,1)S(1)} all-to-all(bf16[8,32,256]{2,1,0:T(8,128)(2,1)S(1)} %broadcast_in_dim.64), channel_id=1, replica_groups=mesh['z'=8,'y'=4,'c'=2,'x'=4] {'z'}, dimensions={0} | all-to-all | bytes 262144 | tf_op jit(solution)/shard_map/all_to_all | solution.py:20
  14.1 11.3 %all_to_all.101 = bf16[8,32,256]{2,1,0:T(8,128)(2,1)S(1)} all-to-all(bf16[8,32,256]{2,1,0:T(8,128)(2,1)S(1)} %broadcast_in_dim.69), channel_id=1, replica_groups=mesh['z'=8,'y'=4,'c'=2,'x'=4] {'z'}, dimensions={0} | all-to-all | bytes 262144 | tf_op jit(solution)/shard_map/all_to_all | solution.py:20
  26.1 6.7 %all-to-all-start.17 = ((bf16[8,32,256]{2,1,0:T(8,128)(2,1)}), bf16[8,32,256]{2,1,0:T(8,128)(2,1)S(1)}, u32[]{:S(2)}, u32[]{:S(2)}) async-start(bf16[8,32,256]{2,1,0:T(8,128)(2,1)} %broadcast_in_dim.74), calls=%async_computation.17 | async-start | bytes 262144 | tf_op jit(solution)/shard_map/all_to_all | solution.py:20
  34.8 0.9 pad_maximum_fusion.1
  35.7 2.7 all-to-all-done.17
  38.5 0.8 broadcast_in_dim.63
  39.3 4.3 %all-to-all-start.4 = ((f32[4,3,34,256]{3,2,1,0:T(8,128)}), f32[4,3,34,256]{3,2,1,0:T(8,128)S(1)}, u32[]{:S(2)}, u32[]{:S(2)}) async-start(f32[4,3,34,256]{3,2,1,0:T(8,128)} %broadcast_in_dim.63), calls=%async_computation.4 | async-start | bytes 983040 | tf_op jit(solution)/shard_map/all_to_all | solution.py:20
  43.6 7.9 %all-to-all-done.4.par = f32[4,3,34,256]{3,2,1,0:T(8,128)S(1)} async-done(((f32[4,3,34,256]{3,2,1,0:T(8,128)}), f32[4,3,34,256]{3,2,1,0:T(8,128)S(1)}, u32[]{:S(2)}, u32[]{:S(2)}) %all-to-all-start.4) | async-done | bytes 417824 | tf_op jit(solution)/shard_map/all_to_all | solution.py:20
  52.2 6.7 %all-to-all-start.1 = ((bf16[8,32,512]{2,1,0:T(8,128)(2,1)}), bf16[8,32,512]{2,1,0:T(8,128)(2,1)S(1)}, u32[]{:S(2)}, u32[]{:S(2)}) async-start(bf16[8,32,512]{2,1,0:T(8,128)(2,1)} %broadcast_in_dim.58), calls=%async_computation.1 | async-start | bytes 524288 | tf_op jit(solution)/shard_map/all_to_all | solution.py:20
  59.0 7.2 %all-to-all-done.1 = bf16[8,32,512]{2,1,0:T(8,128)(2,1)S(1)} async-done(((bf16[8,32,512]{2,1,0:T(8,128)(2,1)}), bf16[8,32,512]{2,1,0:T(8,128)(2,1)S(1)}, u32[]{:S(2)}, u32[]{:S(2)}) %all-to-all-start.1) | async-done | bytes 262176 | tf_op jit(solution)/shard_map/all_to_all | solution.py:20
  66.9 6.6 %all-to-all-start.8 = ((bf16[8,32,512]{2,1,0:T(8,128)(2,1)}), bf16[8,32,512]{2,1,0:T(8,128)(2,1)S(1)}, u32[]{:S(2)}, u32[]{:S(2)}) async-start(bf16[8,32,512]{2,1,0:T(8,128)(2,1)} %broadcast_in_dim.67), calls=%async_computation.8 | async-start | bytes 524288 | tf_op jit(solution)/shard_map/all_to_all | solution.py:20
  73.5 7.2 %all-to-all-done.8 = bf16[8,32,512]{2,1,0:T(8,128)(2,1)S(1)} async-done(((bf16[8,32,512]{2,1,0:T(8,128)(2,1)}), bf16[8,32,512]{2,1,0:T(8,128)(2,1)S(1)}, u32[]{:S(2)}, u32[]{:S(2)}) %all-to-all-start.8) | async-done | bytes 262176 | tf_op jit(solution)/shard_map/all_to_all | solution.py:20
  80.7 13.0 %all_to_all.102 = bf16[8,32,512]{2,1,0:T(8,128)(2,1)S(1)} all-to-all(bf16[8,32,512]{2,1,0:T(8,128)(2,1)S(1)} %broadcast_in_dim.72), channel_id=1, replica_groups=mesh['z'=8,'y'=4,'c'=2,'x'=4] {'z'}, dimensions={0} | all-to-all | bytes 524288 | tf_op jit(solution)/shard_map/all_to_all | solution.py:20
  93.8 13.2 %all_to_all.103 = bf16[4,8,32,256]{3,2,1,0:T(8,128)(2,1)S(1)} all-to-all(bf16[4,8,32,256]{3,2,1,0:T(8,128)(2,1)S(1)} %broadcast_in_dim.65), channel_id=1, replica_groups=mesh['z'=8,'y'=4,'c'=2,'x'=4] {'y'}, dimensions={0} | all-to-all | bytes 1048576 | tf_op jit(solution)/shard_map/all_to_all | solution.py:20
  107.0 13.0 %all_to_all.104 = bf16[4,8,32,256]{3,2,1,0:T(8,128)(2,1)} all-to-all(bf16[4,8,32,256]{3,2,1,0:T(8,128)(2,1)S(1)} %broadcast_in_dim.70), channel_id=1, replica_groups=mesh['z'=8,'y'=4,'c'=2,'x'=4] {'y'}, dimensions={0} | all-to-all | bytes 1048576 | tf_op jit(solution)/shard_map/all_to_all | solution.py:20
  120.1 14.0 %all_to_all.105 = bf16[4,8,32,256]{3,2,1,0:T(8,128)(2,1)} all-to-all(bf16[4,8,32,256]{3,2,1,0:T(8,128)(2,1)S(1)} %broadcast_in_dim.75), channel_id=1, replica_groups=mesh['z'=8,'y'=4,'c'=2,'x'=4] {'y'}, dimensions={0} | all-to-all | bytes 1048576 | tf_op jit(solution)/shard_map/all_to_all | solution.py:20
  134.2 18.2 %all_to_all.106.own = bf16[4,8,32,512]{3,2,1,0:T(8,128)(2,1)} all-to-all(bf16[4,8,32,512]{3,2,1,0:T(8,128)(2,1)S(1)} %broadcast_in_dim.59), channel_id=1, replica_groups=mesh['z'=8,'y'=4,'c'=2,'x'=4] {'y'}, dimensions={0} | all-to-all | bytes 2097152 | tf_op jit(solution)/shard_map/all_to_all | solution.py:20
  152.5 1.1 broadcast_in_dim.68
  153.6 5.6 %all-to-all-start.9 = ((bf16[4,8,32,512]{3,2,1,0:T(8,128)(2,1)}), bf16[4,8,32,512]{3,2,1,0:T(8,128)(2,1)S(1)}, u32[]{:S(2)}, u32[]{:S(2)}) async-start(bf16[4,8,32,512]{3,2,1,0:T(8,128)(2,1)} %broadcast_in_dim.68), calls=%async_computation.9 | async-start | bytes 2097152 | tf_op jit(solution)/shard_map/all_to_all | solution.py:20
  159.2 1.9 collective-permute-start
  161.1 3.6 collective-permute-start.1
  165.1 1.5 collective-permute-done.1
  166.6 1.3 all-to-all-done.9.own
  168.1 28.5 %all_to_all.107.stream = bf16[4,480,512]{2,1,0:T(8,128)(2,1)} all-to-all(bf16[4,480,512]{2,1,0:T(8,128)(2,1)S(1)} %broadcast_in_dim.57), channel_id=1, replica_groups=mesh['z'=8,'y'=4,'c'=2,'x'=4] {'x'}, dimensions={0} | all-to-all | bytes 3932160 | tf_op jit(solution)/shard_map/all_to_all | solution.py:20
  196.9 30.3 %all_to_all.108.own = bf16[4,4,8,32,256]{4,3,2,1,0:T(8,128)(2,1)S(1)} all-to-all(bf16[4,4,8,32,256]{4,3,2,1,0:T(8,128)(2,1)S(1)} %broadcast_in_dim.66), channel_id=1, replica_groups=mesh['z'=8,'y'=4,'c'=2,'x'=4] {'x'}, dimensions={0} | all-to-all | bytes 4194304 | tf_op jit(solution)/shard_map/all_to_all | solution.py:20
  227.2 1.8 broadcast_in_dim.71
  229.1 4.4 %all-to-all-start.13 = ((bf16[4,4,8,32,256]{4,3,2,1,0:T(8,128)(2,1)}), bf16[4,4,8,32,256]{4,3,2,1,0:T(8,128)(2,1)}, u32[]{:S(2)}, u32[]{:S(2)}) async-start(bf16[4,4,8,32,256]{4,3,2,1,0:T(8,128)(2,1)} %broadcast_in_dim.71), calls=%async_computation.13 | async-start | bytes 4194304 | tf_op jit(solution)/shard_map/all_to_all | solution.py:20
  234.7 1.9 collective-permute-done.2.other
  236.6 4.9 %up_0.1 = bf16[4,480,256]{2,1,0:T(8,128)(2,1)} custom-call(s32[5]{0:T(128)} %stack.23.info, bf16[4,480,512]{2,1,0:T(8,128)(2,1)} %all_to_all.107.stream, f32[3,2048]{1,0:T(4,128)} %gain.5, bf16[4,8,32,512]{3,2,1,0:T(8,128)(2,1)} %all_to_all.106.own, bf16[4,8,32,512]{3,2,1,0:T(8,128)(2,1)} %collective-permute-done.2.other), custom_call_target="tpu_custom_call" | custom-call | tf_op jit(solution)/shard_map/up_0/pallas_call | solution.py:136
  241.5 18.9 %all-to-all-done.13.own = bf16[4,4,8,32,256]{4,3,2,1,0:T(8,128)(2,1)} async-done(((bf16[4,4,8,32,256]{4,3,2,1,0:T(8,128)(2,1)}), bf16[4,4,8,32,256]{4,3,2,1,0:T(8,128)(2,1)}, u32[]{:S(2)}, u32[]{:S(2)}) %all-to-all-start.13) | async-done | bytes 2097184 | tf_op jit(solution)/shard_map/all_to_all | solution.py:20
  260.4 4.2 %all-to-all-start.3 = ((bf16[4,480,256]{2,1,0:T(8,128)(2,1)}), bf16[4,480,256]{2,1,0:T(8,128)(2,1)}, u32[]{:S(2)}, u32[]{:S(2)}) async-start(bf16[4,480,256]{2,1,0:T(8,128)(2,1)} %up_0.1), calls=%async_computation.3 | async-start | bytes 1966080 | tf_op jit(solution)/shard_map/all_to_all | solution.py:205
  265.2 13.5 %all-to-all-done.3.gated = bf16[4,480,256]{2,1,0:T(8,128)(2,1)} async-done(((bf16[4,480,256]{2,1,0:T(8,128)(2,1)}), bf16[4,480,256]{2,1,0:T(8,128)(2,1)}, u32[]{:S(2)}, u32[]{:S(2)}) %all-to-all-start.3) | async-done | bytes 983072 | tf_op jit(solution)/shard_map/all_to_all | solution.py:205
  278.7 1.1 broadcast_in_dim.73
  279.8 4.5 %all-to-all-start.15 = ((bf16[4,8,32,512]{3,2,1,0:T(8,128)(2,1)}), bf16[4,8,32,512]{3,2,1,0:T(8,128)(2,1)}, u32[]{:S(2)}, u32[]{:S(2)}) async-start(bf16[4,8,32,512]{3,2,1,0:T(8,128)(2,1)} %broadcast_in_dim.73), calls=%async_computation.15 | async-start | bytes 2097152 | tf_op jit(solution)/shard_map/all_to_all | solution.py:20
  284.3 14.0 %down_0.1.stream = bf16[4,448,512]{2,1,0:T(8,128)(2,1)} custom-call(s32[5]{0:T(128)} %stack.23.info, bf16[4,480,256]{2,1,0:T(8,128)(2,1)} %all-to-all-done.3.gated, f32[4,3,34,256]{3,2,1,0:T(8,128)} %copy-done.1, bf16[4,4,8,32,256]{4,3,2,1,0:T(8,128)(2,1)} %copy-done, bf16[4,4,8,32,256]{4,3,2,1,0:T(8,128)(2,1)} %collective-permute-done.3.other, ...), custom_call_target="tpu_custom_call" | custom-call | tf_op jit(solution)/shard_map/down_0/pallas_call | solution.py:156
  298.3 4.7 %up_1.1 = bf16[4,448,256]{2,1,0:T(8,128)(2,1)} custom-call(s32[5]{0:T(128)} %stack.23.info, bf16[4,448,512]{2,1,0:T(8,128)(2,1)} %down_0.1.stream, f32[3,2048]{1,0:T(4,128)} %gain.5, bf16[4,8,32,512]{3,2,1,0:T(8,128)(2,1)} %copy-done.2, bf16[4,8,32,512]{3,2,1,0:T(8,128)(2,1)} %collective-permute-done.4.other), custom_call_target="tpu_custom_call" | custom-call | tf_op jit(solution)/shard_map/up_1/pallas_call | solution.py:136
  303.0 3.6 all-to-all-start.10
  306.9 0.8 copy.18
  307.8 11.1 %all-to-all-done.10.gated = bf16[4,448,256]{2,1,0:T(8,128)(2,1)S(1)} async-done(((bf16[4,448,256]{2,1,0:T(8,128)(2,1)}), bf16[4,448,256]{2,1,0:T(8,128)(2,1)S(1)}, u32[]{:S(2)}, u32[]{:S(2)}) %all-to-all-start.10) | async-done | bytes 917536 | tf_op jit(solution)/shard_map/all_to_all | solution.py:205
  318.8 3.5 all-to-all-start.19
  322.3 14.2 %down_1.1.stream = bf16[4,416,512]{2,1,0:T(8,128)(2,1)} custom-call(s32[5]{0:T(128)} %stack.23.info, bf16[4,448,256]{2,1,0:T(8,128)(2,1)} %copy-done.3, f32[4,3,34,256]{3,2,1,0:T(8,128)} %copy-done.1, bf16[4,4,8,32,256]{4,3,2,1,0:T(8,128)(2,1)} %all-to-all-done.13.own, bf16[4,4,8,32,256]{4,3,2,1,0:T(8,128)(2,1)} %collective-permute-done.5.other, ...), custom_call_target="tpu_custom_call" | custom-call | tf_op jit(solution)/shard_map/down_1/pallas_call | solution.py:156
  336.5 1.0 copy-done.8
  337.5 4.6 %up_2.1 = bf16[4,416,256]{2,1,0:T(8,128)(2,1)} custom-call(s32[5]{0:T(128)} %stack.23.info, bf16[4,416,512]{2,1,0:T(8,128)(2,1)} %down_1.1.stream, f32[3,2048]{1,0:T(4,128)} %gain.5, bf16[4,8,32,512]{3,2,1,0:T(8,128)(2,1)} %all-to-all-done.15.own, bf16[4,8,32,512]{3,2,1,0:T(8,128)(2,1)} %copy-done.8), custom_call_target="tpu_custom_call" | custom-call | tf_op jit(solution)/shard_map/up_2/pallas_call | solution.py:136
  342.0 4.7 %all-to-all-start.16 = ((bf16[4,416,256]{2,1,0:T(8,128)(2,1)}), bf16[4,416,256]{2,1,0:T(8,128)(2,1)S(1)}, u32[]{:S(2)}, u32[]{:S(2)}) async-start(bf16[4,416,256]{2,1,0:T(8,128)(2,1)} %up_2.1), calls=%async_computation.16 | async-start | bytes 1703936 | tf_op jit(solution)/shard_map/all_to_all | solution.py:205
  346.8 1.9 collective-permute-done.7.other
  348.7 7.9 %all-to-all-done.16.gated = bf16[4,416,256]{2,1,0:T(8,128)(2,1)S(1)} async-done(((bf16[4,416,256]{2,1,0:T(8,128)(2,1)}), bf16[4,416,256]{2,1,0:T(8,128)(2,1)S(1)}, u32[]{:S(2)}, u32[]{:S(2)}) %all-to-all-start.16) | async-done | bytes 852000 | tf_op jit(solution)/shard_map/all_to_all | solution.py:205
  356.6 0.9 copy-done.4
  357.5 9.5 %down_2.1 = bf16[384,512]{1,0:T(8,128)(2,1)} custom-call(s32[5]{0:T(128)} %stack.23.info, bf16[4,416,256]{2,1,0:T(8,128)(2,1)} %copy-done.4, f32[4,3,34,256]{3,2,1,0:T(8,128)} %copy-done.1, bf16[4,4,2,32,256]{4,3,2,1,0:T(8,128)(2,1)} %copy-done.6, bf16[4,4,2,32,256]{4,3,2,1,0:T(8,128)(2,1)} %copy-done.10, bf16[4,416,512]{2,1,0:T(8,128)(2,1)} %down_1.1.stream), custom_call_target="tpu_custom_call" | custom-call | tf_op jit(solution)/shard_map/down_2/pallas_call | solution.py:156
  (60 shorter events, 8.3 us)
Async XLA Ops:
  0.0 43.6 %copy-start.12 = (bf16[3,32,256]{2,1,0:T(8,128)(2,1)S(1)}, bf16[3,32,256]{2,1,0:T(8,128)(2,1)}, u32[]{:S(2)}) copy-start(bf16[3,32,256]{2,1,0:T(8,128)(2,1)} %param.11) | copy-start | bytes 147460
  0.0 43.6 %copy-start.11 = (bf16[3,32,256]{2,1,0:T(8,128)(2,1)S(1)}, bf16[3,32,256]{2,1,0:T(8,128)(2,1)}, u32[]{:S(2)}) copy-start(bf16[3,32,256]{2,1,0:T(8,128)(2,1)} %param.12) | copy-start | bytes 147460
  26.1 12.4 %all-to-all-start.17 = ((bf16[8,32,256]{2,1,0:T(8,128)(2,1)}), bf16[8,32,256]{2,1,0:T(8,128)(2,1)S(1)}, u32[]{:S(2)}, u32[]{:S(2)}) async-start(bf16[8,32,256]{2,1,0:T(8,128)(2,1)} %broadcast_in_dim.74), calls=%async_computation.17 | async-start | bytes 262144 | tf_op jit(solution)/shard_map/all_to_all | solution.py:20
  39.3 12.2 %all-to-all-start.4 = ((f32[4,3,34,256]{3,2,1,0:T(8,128)}), f32[4,3,34,256]{3,2,1,0:T(8,128)S(1)}, u32[]{:S(2)}, u32[]{:S(2)}) async-start(f32[4,3,34,256]{3,2,1,0:T(8,128)} %broadcast_in_dim.63), calls=%async_computation.4 | async-start | bytes 983040 | tf_op jit(solution)/shard_map/all_to_all | solution.py:20
  51.5 55.5 %copy-start.1 = (f32[4,3,34,256]{3,2,1,0:T(8,128)}, f32[4,3,34,256]{3,2,1,0:T(8,128)S(1)}, u32[]{:S(2)}) copy-start(f32[4,3,34,256]{3,2,1,0:T(8,128)S(1)} %all-to-all-done.4.par) | copy-start | bytes 1253380
  52.2 13.9 %all-to-all-start.1 = ((bf16[8,32,512]{2,1,0:T(8,128)(2,1)}), bf16[8,32,512]{2,1,0:T(8,128)(2,1)S(1)}, u32[]{:S(2)}, u32[]{:S(2)}) async-start(bf16[8,32,512]{2,1,0:T(8,128)(2,1)} %broadcast_in_dim.58), calls=%async_computation.1 | async-start | bytes 524288 | tf_op jit(solution)/shard_map/all_to_all | solution.py:20
  66.9 13.8 %all-to-all-start.8 = ((bf16[8,32,512]{2,1,0:T(8,128)(2,1)}), bf16[8,32,512]{2,1,0:T(8,128)(2,1)S(1)}, u32[]{:S(2)}, u32[]{:S(2)}) async-start(bf16[8,32,512]{2,1,0:T(8,128)(2,1)} %broadcast_in_dim.67), calls=%async_computation.8 | async-start | bytes 524288 | tf_op jit(solution)/shard_map/all_to_all | solution.py:20
  152.5 6.7 %copy-start.9 = (bf16[384,512]{1,0:T(8,128)(2,1)S(1)}, bf16[384,512]{1,0:T(8,128)(2,1)}, u32[]{:S(2)}) copy-start(bf16[384,512]{1,0:T(8,128)(2,1)} %param.9) | copy-start | bytes 1179652
  153.6 14.4 %all-to-all-start.9 = ((bf16[4,8,32,512]{3,2,1,0:T(8,128)(2,1)}), bf16[4,8,32,512]{3,2,1,0:T(8,128)(2,1)S(1)}, u32[]{:S(2)}, u32[]{:S(2)}) async-start(bf16[4,8,32,512]{3,2,1,0:T(8,128)(2,1)} %broadcast_in_dim.68), calls=%async_computation.9 | async-start | bytes 2097152 | tf_op jit(solution)/shard_map/all_to_all | solution.py:20
  159.2 5.9 %collective-permute-start = (bf16[48,512]{1,0:T(8,128)(2,1)S(1)}, bf16[48,512]{1,0:T(8,128)(2,1)S(1)}, u32[]{:S(2)}, u32[]{:S(2)}) collective-permute-start(bf16[48,512]{1,0:T(8,128)(2,1)S(1)} %get-tuple-element.5), channel_id=1, source_target_pairs={{0,4},{4,8},{8,12},{12,16},{16,20},{20,24},{24,28},{28,32},{32,36}... | collective-permute-start | bytes 147464 | tf_op jit(solution)/shard_map/ppermute | solution.py:182
  161.1 5.5 %collective-permute-start.1 = (bf16[48,512]{1,0:T(8,128)(2,1)S(1)}, bf16[48,512]{1,0:T(8,128)(2,1)S(1)}, u32[]{:S(2)}, u32[]{:S(2)}) collective-permute-start(bf16[48,512]{1,0:T(8,128)(2,1)S(1)} %get-tuple-element.6), channel_id=1, source_target_pairs={{4,0},{8,4},{12,8},{16,12},{20,16},{24,20},{28,24},{32,28},{36,32}... | collective-permute-start | bytes 147464 | tf_op jit(solution)/shard_map/ppermute | solution.py:183
  168.0 96.6 %copy-start.2 = (bf16[4,8,32,512]{3,2,1,0:T(8,128)(2,1)}, bf16[4,8,32,512]{3,2,1,0:T(8,128)(2,1)S(1)}, u32[]{:S(2)}) copy-start(bf16[4,8,32,512]{3,2,1,0:T(8,128)(2,1)S(1)} %all-to-all-done.9.own) | copy-start | bytes 3145732
  196.9 30.3 %copy-start.5 = (bf16[4,8,32,256]{3,2,1,0:T(8,128)(2,1)S(1)}, bf16[4,8,32,256]{3,2,1,0:T(8,128)(2,1)}, u32[]{:S(2)}) copy-start(bf16[4,8,32,256]{3,2,1,0:T(8,128)(2,1)} %all_to_all.104) | copy-start | bytes 1572868
  227.2 6.4 %copy-start = (bf16[4,4,8,32,256]{4,3,2,1,0:T(8,128)(2,1)}, bf16[4,4,8,32,256]{4,3,2,1,0:T(8,128)(2,1)S(1)}, u32[]{:S(2)}) copy-start(bf16[4,4,8,32,256]{4,3,2,1,0:T(8,128)(2,1)S(1)} %all_to_all.108.own) | copy-start | bytes 6291460
  229.1 31.3 %all-to-all-start.13 = ((bf16[4,4,8,32,256]{4,3,2,1,0:T(8,128)(2,1)}), bf16[4,4,8,32,256]{4,3,2,1,0:T(8,128)(2,1)}, u32[]{:S(2)}, u32[]{:S(2)}) async-start(bf16[4,4,8,32,256]{4,3,2,1,0:T(8,128)(2,1)} %broadcast_in_dim.71), calls=%async_computation.13 | async-start | bytes 4194304 | tf_op jit(solution)/shard_map/all_to_all | solution.py:20
  233.5 3.1 collective-permute-start.2
  233.6 50.7 %collective-permute-start.3 = (bf16[4,4,8,32,256]{4,3,2,1,0:T(8,128)(2,1)S(1)}, bf16[4,4,8,32,256]{4,3,2,1,0:T(8,128)(2,1)}, u32[]{:S(2)}, u32[]{:S(2)}) collective-permute-start(bf16[4,4,8,32,256]{4,3,2,1,0:T(8,128)(2,1)S(1)} %all_to_all.108.own), channel_id=1, source_target_pairs={{0,4},{4,0},{1,5},{5,1},{2,6},{6,2},{3,7},{7,3},{8,12},{12,8},{9,1... | collective-permute-start | bytes 6291464 | tf_op jit(solution)/shard_map/ppermute | solution.py:24
  260.4 18.3 %all-to-all-start.3 = ((bf16[4,480,256]{2,1,0:T(8,128)(2,1)}), bf16[4,480,256]{2,1,0:T(8,128)(2,1)}, u32[]{:S(2)}, u32[]{:S(2)}) async-start(bf16[4,480,256]{2,1,0:T(8,128)(2,1)} %up_0.1), calls=%async_computation.3 | async-start | bytes 1966080 | tf_op jit(solution)/shard_map/all_to_all | solution.py:205
  264.6 33.6 %collective-permute-start.4 = (bf16[4,8,32,512]{3,2,1,0:T(8,128)(2,1)S(1)}, bf16[4,8,32,512]{3,2,1,0:T(8,128)(2,1)}, u32[]{:S(2)}, u32[]{:S(2)}) collective-permute-start(bf16[4,8,32,512]{3,2,1,0:T(8,128)(2,1)S(1)} %all-to-all-done.9.own), channel_id=1, source_target_pairs={{0,4},{4,0},{1,5},{5,1},{2,6},{6,2},{3,7},{7,3},{8,12},{12,8},{9,1... | collective-permute-start | bytes 3145736 | tf_op jit(solution)/shard_map/ppermute | solution.py:24
  264.7 57.6 %collective-permute-start.5 = (bf16[4,4,8,32,256]{4,3,2,1,0:T(8,128)(2,1)}, bf16[4,4,8,32,256]{4,3,2,1,0:T(8,128)(2,1)}, u32[]{:S(2)}, u32[]{:S(2)}) collective-permute-start(bf16[4,4,8,32,256]{4,3,2,1,0:T(8,128)(2,1)} %all-to-all-done.13.own), channel_id=1, source_target_pairs={{0,4},{4,0},{1,5},{5,1},{2,6},{6,2},{3,7},{7,3},{8,12},{12,8},{9,1... | collective-permute-start | bytes 6291464 | tf_op jit(solution)/shard_map/ppermute | solution.py:24
  279.8 23.2 %all-to-all-start.15 = ((bf16[4,8,32,512]{3,2,1,0:T(8,128)(2,1)}), bf16[4,8,32,512]{3,2,1,0:T(8,128)(2,1)}, u32[]{:S(2)}, u32[]{:S(2)}) async-start(bf16[4,8,32,512]{3,2,1,0:T(8,128)(2,1)} %broadcast_in_dim.73), calls=%async_computation.15 | async-start | bytes 2097152 | tf_op jit(solution)/shard_map/all_to_all | solution.py:20
  303.0 3.9 %copy-start.7 = (bf16[4,8,32,256]{3,2,1,0:T(8,128)(2,1)S(1)}, bf16[4,8,32,256]{3,2,1,0:T(8,128)(2,1)}, u32[]{:S(2)}) copy-start(bf16[4,8,32,256]{3,2,1,0:T(8,128)(2,1)} %all_to_all.105) | copy-start | bytes 1572868
  303.0 15.8 %all-to-all-start.10 = ((bf16[4,448,256]{2,1,0:T(8,128)(2,1)}), bf16[4,448,256]{2,1,0:T(8,128)(2,1)S(1)}, u32[]{:S(2)}, u32[]{:S(2)}) async-start(bf16[4,448,256]{2,1,0:T(8,128)(2,1)} %up_1.1), calls=%async_computation.10 | async-start | bytes 1835008 | tf_op jit(solution)/shard_map/all_to_all | solution.py:205
  306.6 29.9 %collective-permute-start.6 = (bf16[4,8,32,512]{3,2,1,0:T(8,128)(2,1)}, bf16[4,8,32,512]{3,2,1,0:T(8,128)(2,1)S(1)}, u32[]{:S(2)}, u32[]{:S(2)}) collective-permute-start(bf16[4,8,32,512]{3,2,1,0:T(8,128)(2,1)} %all-to-all-done.15.own), channel_id=1, source_target_pairs={{0,4},{4,0},{1,5},{5,1},{2,6},{6,2},{3,7},{7,3},{8,12},{12,8},{9,1... | collective-permute-start | bytes 3145736 | tf_op jit(solution)/shard_map/ppermute | solution.py:24
  318.8 3.5 copy-start.3
  318.8 23.2 %all-to-all-start.19 = ((bf16[4,4,2,32,256]{4,3,2,1,0:T(8,128)(2,1)}), bf16[4,4,2,32,256]{4,3,2,1,0:T(8,128)(2,1)S(1)}, u32[]{:S(2)}, u32[]{:S(2)}) async-start(bf16[4,4,2,32,256]{4,3,2,1,0:T(8,128)(2,1)} %bitcast.30), calls=%async_computation.19 | async-start | bytes 1048576 | tf_op jit(solution)/shard_map/all_to_all | solution.py:199
  336.5 1.0 copy-start.8
  342.0 14.6 %copy-start.6 = (bf16[4,4,2,32,256]{4,3,2,1,0:T(8,128)(2,1)}, bf16[4,4,2,32,256]{4,3,2,1,0:T(8,128)(2,1)S(1)}, u32[]{:S(2)}) copy-start(bf16[4,4,2,32,256]{4,3,2,1,0:T(8,128)(2,1)S(1)} %all-to-all-done.19.own) | copy-start | bytes 1572868
  342.0 14.6 %all-to-all-start.16 = ((bf16[4,416,256]{2,1,0:T(8,128)(2,1)}), bf16[4,416,256]{2,1,0:T(8,128)(2,1)S(1)}, u32[]{:S(2)}, u32[]{:S(2)}) async-start(bf16[4,416,256]{2,1,0:T(8,128)(2,1)} %up_2.1), calls=%async_computation.16 | async-start | bytes 1703936 | tf_op jit(solution)/shard_map/all_to_all | solution.py:205
  346.8 1.9 collective-permute-start.7
  348.7 7.9 %copy-start.10 = (bf16[4,4,2,32,256]{4,3,2,1,0:T(8,128)(2,1)}, bf16[4,4,2,32,256]{4,3,2,1,0:T(8,128)(2,1)S(1)}, u32[]{:S(2)}) copy-start(bf16[4,4,2,32,256]{4,3,2,1,0:T(8,128)(2,1)S(1)} %collective-permute-done.7.other) | copy-start | bytes 1572868
  356.6 0.9 copy-start.4
